TPU v7x, 32 devices: a whole 2x2x4 slice. The times are simulated.
32 devices in a mesh: rep: 2 (over x), fs: 8 (over z, y), tp: 2 (over core).
Axes of the slice: x: 2, y: 2, z: 4, core: 2. Of those that a mesh axis runs over, the one named last changes fastest.
Arguments:
- stream: bfloat16 [16, 1024, 2048], P(('rep', 'fs'), None, 'tp'), may hold values from -6 to 6
- norm_gain: float32 [2048], replicated, may hold values from 0.1 to 1.9
- w_in: float32 [2048, 512], P('fs', 'tp'), may hold values from -0.125 to 0.125
- s_in: float32 [512], P(('tp', 'fs')), may hold values from 0.1 to 1.9
- pool_w: bfloat16 [4, 128, 128], replicated, may hold values from -0.5 to 0.5
- w_out: float32 [512, 2048], P('fs', 'tp'), may hold values from -0.25 to 0.25
- s_out: float32 [2048], P(('tp', 'fs')), may hold values from 0.1 to 1.9
- ffn_gain: float32 [2048], replicated, may hold values from 0.1 to 1.9
- w_up: float32 [2048, 8192], P('fs', 'tp'), may hold values from -0.125 to 0.125
- s_up: float32 [8192], P(('tp', 'fs')), may hold values from 0.1 to 1.9
- w_down: float32 [8192, 2048], P('tp', 'fs'), may hold values from -0.0625 to 0.0625
- s_down: float32 [2048], P('fs'), may hold values from 0.1 to 1.9
Outputs:
- result: bfloat16 [16, 1024, 2048], P(('rep', 'fs'), None, 'tp')
All inputs are finite; a program needn't handle non-finite values.
Results may differ from a plain program's by a relative error of at most 0.012.
Values may be sent and summed in bfloat16 or wider, within the bound.
A program may use at most 128 MiB of HBM per device.

v0:
```python
import jax
import jax.numpy as jnp
from jax import lax
from jax.sharding import PartitionSpec as P

PW = 512
GROUP = 128


epsilon = 0.25


def rms_rows(values, gain):
    floats = values.astype(jnp.float32)
    scale = lax.rsqrt(jnp.mean(floats * floats, axis=-1, keepdims=True) + epsilon)
    return (floats * scale * gain).astype(jnp.bfloat16)


def pool_local(pool_in, first):
    length, width = pool_in.shape
    positions = jnp.arange(length, dtype=jnp.int32)
    source = positions[None, :]
    target = positions[:, None]
    group_of = (first + jnp.arange(width, dtype=jnp.int32)) // GROUP
    means = jnp.zeros((length, width), jnp.float32)
    for level in range(4):
        half = 2**level
        band_ones = ((source >= target - half) & (source < target + half)).astype(jnp.bfloat16)
        counts = (jnp.minimum(positions + half, length) - jnp.maximum(positions - half, 0)).astype(
            jnp.float32
        )
        sums = jnp.dot(band_ones, pool_in, preferred_element_type=jnp.float32) / counts[:, None]
        means = jnp.where(group_of[None, :] == level, sums, means)
    return (means - pool_in.astype(jnp.float32)).astype(jnp.bfloat16)


def fold_rows(left, piece):
    return jnp.dot(left, piece, preferred_element_type=jnp.float32)


def on_device(
    stream, norm_gain, w_in, s_in, pool_w, w_out, s_out, ffn_gain, w_up, s_up, w_down, s_down
):
    tokens = stream[0]
    length = tokens.shape[0]
    scale_in, scale_out, scale_up, scale_down = (
        lax.all_gather(s_in, "fs", axis=0, tiled=True),
        lax.all_gather(s_out, "fs", axis=0, tiled=True),
        lax.all_gather(s_up, "fs", axis=0, tiled=True),
        lax.all_gather(s_down, "fs", axis=0, tiled=True),
    )
    full_rows = lax.all_gather(tokens, "tp", axis=1, tiled=True)
    normed = rms_rows(full_rows, norm_gain)
    projected = fold_rows(
        normed, lax.all_gather(w_in.astype(jnp.bfloat16), "fs", axis=0, tiled=True)
    )
    pool_in = (projected * scale_in).astype(jnp.bfloat16)
    pooled = pool_local(pool_in, lax.axis_index("tp") * pool_in.shape[1])
    pooled_all = lax.all_gather(pooled, "tp", axis=1, tiled=True)
    grouped = jnp.einsum(
        "lgc,gcd->lgd",
        pooled_all.reshape(length, 4, GROUP),
        pool_w,
        preferred_element_type=jnp.float32,
    )
    grouped = grouped.reshape(length, PW).astype(jnp.bfloat16)
    branch = fold_rows(
        grouped, lax.all_gather(w_out.astype(jnp.bfloat16), "fs", axis=0, tiled=True)
    )
    mixed = (tokens.astype(jnp.float32) + branch * scale_out).astype(jnp.bfloat16)
    mixed_full = lax.all_gather(mixed, "tp", axis=1, tiled=True)
    ffn_in = rms_rows(mixed_full, ffn_gain)
    upward = fold_rows(ffn_in, lax.all_gather(w_up.astype(jnp.bfloat16), "fs", axis=0, tiled=True))
    hidden = jnp.square(jax.nn.relu(upward * scale_up)).astype(jnp.bfloat16)
    partial_value = jnp.dot(
        hidden,
        lax.all_gather(w_down.astype(jnp.bfloat16), "fs", axis=1, tiled=True),
        preferred_element_type=jnp.float32,
    )
    rounded = lax.optimization_barrier((partial_value * scale_down).astype(jnp.bfloat16))
    summed = lax.psum_scatter(
        rounded.astype(jnp.float32).astype(jnp.bfloat16), "tp", scatter_dimension=1, tiled=True
    ).astype(jnp.float32)
    return (mixed.astype(jnp.float32) + summed).astype(jnp.bfloat16)[None]


def solution(mesh):
    return jax.shard_map(
        on_device,
        mesh=mesh,
        in_specs=(
            P(("rep", "fs"), None, "tp"),
            P(),
            P("fs", "tp"),
            P(("tp", "fs")),
            P(),
            P("fs", "tp"),
            P(("tp", "fs")),
            P(),
            P("fs", "tp"),
            P(("tp", "fs")),
            P("tp", "fs"),
            P("fs"),
        ),
        out_specs=P(("rep", "fs"), None, "tp"),
        check_vma=False,
    )
```

profile of v0, /device:TPU:0, one launch (start us, length us, event | category | flops | bytes accessed | tf_op | source)
XLA Modules:
  0.0 650.5 jit_solution(18114891984723246178)
XLA Ops:
  6.5 0.7 all-gather.24.cloned.1.call-update
  7.3 0.0 all-gather.12.cloned.1.call-start
  7.3 1.6 convert_element_type.100
  8.9 0.0 all-gather.12.cloned.1.call-update
  9.0 0.0 all-gather.14.cloned.1.call-start
  9.0 1.3 dynamic-slice
  10.9 0.9 dynamic-update-slice
  11.8 23.1 %all-reduce = f32[256]{0:T(256)S(1)} all-reduce(f32[256]{0:T(256)S(1)} %dynamic-update-slice), channel_id=1, replica_groups=mesh['rep'=2,'fs'=8,'tp'=2] {'fs'}, use_global_device_ids=true, to_apply=%add | all-reduce | flops 256 | bytes 2048
  35.0 0.0 all-gather.24.cloned.1.call-done
  35.0 3.2 fusion.3
  38.2 30.7 %all-gather.12.cloned.1.call-done = bf16[2048,256]{1,0:T(8,128)(2,1)} async-done(((bf16[256,256]{1,0:T(8,128)(2,1)}), bf16[2048,256]{1,0:T(8,128)(2,1)}) %all-gather.12.cloned.1.call-update) | async-done | bytes 1048592 | tf_op jit(solution)/shard_map/all_gather | solution.py:55
  68.9 3.8 fusion.39
  72.7 1.5 fusion.16
  74.2 1.5 fusion.19
  75.7 1.5 fusion.22
  77.1 0.0 copy-start.4
  77.2 0.0 copy-start.7
  77.2 0.0 copy-start.3
  77.2 2.8 subtract_convert_fusion
  80.0 0.0 all-gather.14.cloned.1.call-update
  80.0 0.0 all-gather.16.cloned.1.call-start
  80.1 0.7 convert_element_type.111
  80.7 0.0 all-gather.16.cloned.1.call-update
  80.8 0.0 all-gather.18.cloned.1.call-start
  80.8 18.3 %all-gather.1 = f32[8,1,128]{2,1,0:T(1,128)S(1)} all-gather(f32[1,1,128]{2,1,0:T(1,128)S(1)} %bitcast.54), channel_id=1, replica_groups=mesh['rep'=2,'fs'=8,'tp'=2] {'fs'}, dimensions={0}, use_global_device_ids=true | all-gather | bytes 4608 | tf_op jit(solution)/shard_map/all_gather | solution.py:48
  99.1 1.7 convolution_convert_fusion
  100.8 30.3 %all-gather.16.cloned.1.call-done = bf16[512,1024]{1,0:T(8,128)(2,1)} async-done(((bf16[64,1024]{1,0:T(8,128)(2,1)}), bf16[512,1024]{1,0:T(8,128)(2,1)}) %all-gather.16.cloned.1.call-update) | async-done | bytes 1048592 | tf_op jit(solution)/shard_map/all_gather | solution.py:68
  131.2 3.9 fusion.9
  135.1 0.0 all-gather.18.cloned.1.call-update
  135.1 0.0 all-gather.20.cloned.1.call-start
  135.2 3.8 convert_element_type.116
  138.9 0.0 all-gather.20.cloned.1.call-update
  138.9 0.0 copy-start.6
  139.0 0.0 copy-start.5
  139.0 0.0 all-gather.22.cloned.1.call-start
  139.0 4.2 convert_element_type.118
  143.3 0.0 all-gather.22.cloned.1.call-update
  143.3 0.0 reduce-scatter.2.cloned.1.call-start
  143.3 17.8 %all-gather.3 = f32[8,1,256]{2,1,0:T(1,128)S(1)} all-gather(f32[1,1,256]{2,1,0:T(1,128)S(1)} %bitcast.53), channel_id=1, replica_groups=mesh['rep'=2,'fs'=8,'tp'=2] {'fs'}, dimensions={0}, use_global_device_ids=true | all-gather | bytes 9216 | tf_op jit(solution)/shard_map/all_gather | solution.py:50
  161.1 27.7 %all-gather.2 = f32[8,1,512]{2,1,0:T(1,128)S(1)} all-gather(f32[1,1,512]{2,1,0:T(1,128)S(1)} %bitcast.52), channel_id=1, replica_groups=mesh['rep'=2,'fs'=8,'tp'=2] {'fs'}, dimensions={0}, use_global_device_ids=true | all-gather | bytes 18432 | tf_op jit(solution)/shard_map/all_gather | solution.py:49
  188.8 3.1 fusion
  191.9 186.4 %all-gather.20.cloned.1.call-done = bf16[2048,4096]{1,0:T(8,128)(2,1)} async-done(((bf16[256,4096]{1,0:T(8,128)(2,1)}), bf16[2048,4096]{1,0:T(8,128)(2,1)}) %all-gather.20.cloned.1.call-update) | async-done | bytes 16777232 | tf_op jit(solution)/shard_map/all_gather | solution.py:73
  378.3 23.1 %multiply_convert_fusion.clone.4 = bf16[1024,4096]{1,0:T(8,128)(2,1)} fusion(bf16[2048,4096]{1,0:T(8,128)(2,1)} %all-gather.20.cloned.1.call-done, f32[4096]{0:T(1024)S(1)} %bitcast.49, bf16[1024,2048]{1,0:T(8,128)(2,1)} %all-gather.18.cloned.1.call-done, f32[2048]{0:T(1024)S(1)} %copy-done.9, f32[1024]{0:T(1024)S(1)} %add_rsqrt_fusion), kind=kOutput, calls=%fused_computation.clone.clone.clone.1 | convolution fusion | flops 17205035008 | bytes 29388800 | tf_op jit(solution)/shard_map/dot_general | solution.py:38
  401.4 204.5 %all-gather.22.cloned.1.call-done = bf16[4096,2048]{1,0:T(8,128)(2,1)} async-done(((bf16[4096,256]{1,0:T(8,128)(2,1)}), bf16[4096,2048]{1,0:T(8,128)(2,1)}) %all-gather.22.cloned.1.call-update) | async-done | bytes 16777232 | tf_op jit(solution)/shard_map/all_gather | solution.py:77
  605.9 23.7 %multiply_convert_fusion.1 = bf16[1024,2048]{1,0:T(8,128)(2,1)} fusion(bf16[4096,2048]{1,0:T(8,128)(2,1)} %all-gather.22.cloned.1.call-done, f32[2048]{0:T(1024)S(1)} %bitcast.50, bf16[1024,4096]{1,0:T(8,128)(2,1)} %multiply_convert_fusion.clone.4), kind=kOutput, calls=%fused_computation.11 | convolution fusion | flops 17184063488 | bytes 29368320 | tf_op jit(solution)/shard_map/dot_general | solution.py:75
  629.5 0.0 reduce-scatter.2.cloned.1.call-update
  629.6 10.2 %reduce-scatter.2.cloned.1.call-done = bf16[1024,1024]{1,0:T(8,128)(2,1)} async-done(((bf16[1024,2048]{1,0:T(8,128)(2,1)}), bf16[1024,1024]{1,0:T(8,128)(2,1)}) %reduce-scatter.2.cloned.1.call-update) | async-done | bytes 2097168 | tf_op jit(solution)/shard_map/reduce_scatter | solution.py:81
  639.8 3.9 fusion.27
  (29 shorter events, 0.1 us)
Async XLA Ops:
  6.5 92.6 %copy-start = (bf16[4,128,128]{2,1,0:T(8,128)(2,1)S(1)}, bf16[4,128,128]{2,1,0:T(8,128)(2,1)}, u32[]{:S(2)}) copy-start(bf16[4,128,128]{2,1,0:T(8,128)(2,1)} %param.16) | copy-start | bytes 393220
  6.5 62.4 %copy-start.8 = (f32[2048]{0:T(1024)S(1)}, f32[2048]{0:T(1024)}, u32[]{:S(2)}) copy-start(f32[2048]{0:T(1024)} %param.13) | copy-start | bytes 24580
  6.5 28.5 %all-gather.24.cloned.1.call-start = ((), (), s32[]{:S(2)}) async-start(), calls=%async_computation.8 | async-start | bytes 6291456 | tf_op jit(solution)/shard_map/all_gather | solution.py:52
  7.3 61.6 %all-gather.12.cloned.1.call-start = ((), (), s32[]{:S(2)}) async-start(), calls=%async_computation.1 | async-start | bytes 1179648 | tf_op jit(solution)/shard_map/all_gather | solution.py:55
  9.0 90.2 %all-gather.14.cloned.1.call-start = ((), (), s32[]{:S(2)}) async-start(), calls=%async_computation.2 | async-start | bytes 1572864 | tf_op jit(solution)/shard_map/all_gather | solution.py:59
  77.1 2.9 copy-start.4
  77.2 3.7 copy-start.7
  77.2 54.0 %copy-start.3 = (bf16[1,1024,1024]{2,1,0:T(8,128)(2,1)S(1)}, bf16[1,1024,1024]{2,1,0:T(8,128)(2,1)}, u32[]{:S(2)}) copy-start(bf16[1,1024,1024]{2,1,0:T(8,128)(2,1)} %param.12) | copy-start | bytes 6291460
  80.0 51.1 %all-gather.16.cloned.1.call-start = ((), (), s32[]{:S(2)}) async-start(), calls=%async_computation.3 | async-start | bytes 1179648 | tf_op jit(solution)/shard_map/all_gather | solution.py:68
  80.8 108.0 %all-gather.18.cloned.1.call-start = ((), (), s32[]{:S(2)}) async-start(), calls=%async_computation.4 | async-start | bytes 6291456 | tf_op jit(solution)/shard_map/all_gather | solution.py:71
  135.1 243.2 %all-gather.20.cloned.1.call-start = ((), (), s32[]{:S(2)}) async-start(), calls=%async_computation.5 | async-start | bytes 18874368 | tf_op jit(solution)/shard_map/all_gather | solution.py:73
  138.9 4.4 copy-start.6
  139.0 22.2 %copy-start.5 = (f32[512]{0:T(512)S(1)}, f32[512]{0:T(512)}, u32[]{:S(2)}) copy-start(f32[512]{0:T(512)} %param.21) | copy-start | bytes 6148
  139.0 466.9 %all-gather.22.cloned.1.call-start = ((), (), s32[]{:S(2)}) async-start(), calls=%async_computation.6 | async-start | bytes 18874368 | tf_op jit(solution)/shard_map/all_gather | solution.py:77
  143.3 235.1 %copy-start.9 = (f32[2048]{0:T(1024)S(1)}, f32[2048]{0:T(1024)}, u32[]{:S(2)}) copy-start(f32[2048]{0:T(1024)} %param.19) | copy-start | bytes 24580
  143.3 496.5 %reduce-scatter.2.cloned.1.call-start = ((), (), s32[]{:S(2)}) async-start(), calls=%async_computation.7 | async-start | bytes 6291456 | tf_op jit(solution)/shard_map/reduce_scatter | solution.py:81
  629.5 10.2 %copy-start.2 = (bf16[1024,1024]{1,0:T(8,128)(2,1)S(1)}, bf16[1024,1024]{1,0:T(8,128)(2,1)}, u32[]{:S(2)}) copy-start(bf16[1024,1024]{1,0:T(8,128)(2,1)} %fusion.9) | copy-start | bytes 6291460
  629.6 14.1 %copy-start.1 = (bf16[4,128,128]{2,1,0:T(8,128)(2,1)S(1)}, bf16[4,128,128]{2,1,0:T(8,128)(2,1)}, u32[]{:S(2)}) copy-start(bf16[4,128,128]{2,1,0:T(8,128)(2,1)} %param.16) | copy-start | bytes 393220
Sparse Core Ops, SparseCore 0:
  8.9 16.3 all-gather.23
  27.4 41.4 all-gather.11
  80.1 7.4 all-gather.13
  89.6 41.4 all-gather.15
  135.2 12.3 all-gather.17
  149.6 228.6 all-gather.19
  380.4 225.4 all-gather.21
  629.7 10.0 reduce-scatter.1
where the time goes:
time: 651 us; the launch traced here: 650 us
  waiting for transfers between devices  463 us (71%)
  blocking collectives  86.9 us (13%)
  matrix products  63.4 us (10%)
  other arithmetic  20.5 us (3%)
  between operations  14.3 us (2%)
    all_gather x1, waiting for transfers between devices, on_device(): lax.all_gather(w_down.astype(jnp.bfloat16), 'fs', axis=1, tiled=True)  204 us
    all_gather x1, waiting for transfers between devices, on_device(): lax.all_gather(w_up.astype(jnp.bfloat16), 'fs', axis=0, tiled=True)  186 us
    dot_general x3, matrix products, fold_rows(): return jnp.dot(left, piece, preferred_element_type=jnp.float32)  30.8 us
    all_gather x1, waiting for transfers between devices, on_device(): lax.all_gather(w_in.astype(jnp.bfloat16), 'fs', axis=0, tiled=True)  30.7 us
    all_gather x1, waiting for transfers between devices, on_device(): lax.all_gather(w_out.astype(jnp.bfloat16), 'fs', axis=0, tiled=True)  30.3 us
    all_gather x1, blocking collectives, on_device(): lax.all_gather(s_up, 'fs', axis=0, tiled=True)  27.7 us
    dot_general x1, matrix products, on_device(): jnp.dot(hidden, lax.all_gather(w_down.astype(jnp.bfloat16), 'fs', axis=1,...  23.7 us
    unnamed x1, blocking collectives  23.1 us
  transfers between devices with their start and end apart: 8, of which 5 were waited for; matrix products, arithmetic and copies ran while one was open for 7% of the time, Pallas kernels for 0%

commit v1 on v0

v1 whole, which is shorter than its diff:
```python
import jax
import jax.numpy as jnp
from jax import lax
from jax.sharding import PartitionSpec as P

GROUP = 128


epsilon = 0.25
bf16 = jnp.bfloat16
f32 = jnp.float32


def dot(left, right):
    return jnp.dot(left, right, preferred_element_type=f32)


def rms_rows(values, gain):
    floats = values.astype(f32)
    scale = lax.rsqrt(jnp.mean(floats * floats, axis=-1, keepdims=True) + epsilon)
    return (floats * scale * gain).astype(bf16)


def shifted(value, axis_name, count, offset):
    return lax.ppermute(value, axis_name, [(i, (i + offset) % count) for i in range(count)])


def swap_gather(value, axis_name, count, axis):
    index = lax.axis_index(axis_name)
    width = value.shape[axis]
    shape = list(value.shape)
    shape[axis] = width * count
    if count == 2:
        other = shifted(value, axis_name, count, 1)
        low = jnp.where(index == 0, value, other)
        high = jnp.where(index == 0, other, value)
        return jnp.concatenate([low, high], axis=axis)
    full = jnp.zeros(shape, value.dtype)
    full = lax.dynamic_update_slice_in_dim(full, value, index * width, axis)
    for offset in range(1, count):
        piece = shifted(value, axis_name, count, offset)
        origin = (index - offset) % count
        full = lax.dynamic_update_slice_in_dim(full, piece, origin * width, axis)
    return full


def fs_sent(value, factors, offset_a, offset_b):
    n_a, n_b = factors
    pairs = []
    for i in range(n_a * n_b):
        pairs.append((i, ((i // n_b) ^ offset_a) * n_b + ((i % n_b) ^ offset_b)))
    return lax.ppermute(value, "fs", pairs)


def fs_pieces(value, factors):
    n_a, n_b = factors
    rows = [[value] for _ in range(n_a)]
    for x in range(1, n_a):
        rows[x] = [fs_sent(value, factors, x, 0)]
    for y in range(1, n_b):
        for x in range(n_a):
            rows[x].append(fs_sent(rows[x][0], factors, 0, y))
    return rows


def fs_origin(factors, x, y):
    index = lax.axis_index("fs")
    return ((index // factors[1]) ^ x) * factors[1] + ((index % factors[1]) ^ y)


def placed(rows, factors):
    block = rows[0][0].shape[0]
    width = rows[0][0].shape[1]
    full = jnp.zeros((block * factors[0] * factors[1], width), rows[0][0].dtype)
    for y in range(factors[1]):
        for x in range(factors[0]):
            full = lax.dynamic_update_slice_in_dim(
                full, rows[x][y], fs_origin(factors, x, y) * block, 0
            )
    return full


def pool_local(pool_in, first):
    length, width = pool_in.shape
    positions = jnp.arange(length, dtype=jnp.int32)
    source = positions[None, :]
    target = positions[:, None]
    group_of = (first + jnp.arange(width, dtype=jnp.int32)) // GROUP
    means = jnp.zeros((length, width), f32)
    for level in range(4):
        half = 2**level
        band_ones = ((source >= target - half) & (source < target + half)).astype(bf16)
        counts = (jnp.minimum(positions + half, length) - jnp.maximum(positions - half, 0)).astype(f32)
        sums = dot(band_ones, pool_in) / counts[:, None]
        means = jnp.where(group_of[None, :] == level, sums, means)
    return (means - pool_in.astype(f32)).astype(bf16)


def on_device(
    n_rep, n_fs, n_tp,
    stream, norm_gain, w_in, s_in, pool_w, w_out, s_out, ffn_gain, w_up, s_up, w_down, s_down,
):
    rep = lax.axis_index("rep")
    tokens = stream[0]
    length, local_width = tokens.shape
    hidden_width = w_up.shape[1] // n_rep

    n_a = n_tp * max(1, 4 // n_tp)
    factors = (n_a, n_fs // n_a)

    scales = jnp.concatenate([s_in, s_out, s_up, s_down])[None]
    scale_rows = [
        [scales if x == y == 0 else fs_sent(scales, factors, x, y) for y in range(factors[1])]
        for x in range(n_a)
    ]
    scales = placed(scale_rows, factors)
    ends, at = [], 0
    for part in (s_in, s_out, s_up, s_down):
        ends.append(scales[:, at:at + part.shape[0]])
        at += part.shape[0]
    scale_in, scale_out, scale_up = (part.reshape(-1) for part in ends[:3])
    scale_down = ends[3]

    in_rows = fs_pieces(w_in.astype(bf16), factors)
    out_rows = fs_pieces(w_out.astype(bf16), factors)
    w_in_all = placed(in_rows, factors)
    w_out_all = placed(out_rows, factors)

    up_own = lax.dynamic_slice_in_dim(w_up, rep * hidden_width, hidden_width, 1).astype(bf16)
    up_rows = fs_pieces(up_own, factors)
    up_all = placed(up_rows, factors)
    down_own = lax.dynamic_slice_in_dim(w_down, rep * hidden_width, hidden_width, 0).astype(bf16)
    down_own, *_ = lax.optimization_barrier((down_own, *[in_rows[x][0] for x in range(1, n_a)]))
    down_rows = fs_pieces(down_own, factors)

    normed = rms_rows(swap_gather(tokens, "tp", n_tp, 1), norm_gain)
    pool_in = (dot(normed, w_in_all) * scale_in).astype(bf16)
    pooled = pool_local(pool_in, lax.axis_index("tp") * pool_in.shape[1])
    pooled_all = swap_gather(pooled, "tp", n_tp, 1)
    groups = pool_w.shape[0]
    grouped = jnp.einsum(
        "lgc,gcd->lgd", pooled_all.reshape(length, groups, GROUP), pool_w, preferred_element_type=f32
    ).reshape(length, groups * GROUP).astype(bf16)
    mixed = (tokens.astype(f32) + dot(grouped, w_out_all) * scale_out).astype(bf16)

    mixed_own = swap_gather(mixed, "tp", n_tp, 1)
    sequences = [mixed_own]
    for offset in range(1, n_rep):
        other = shifted(mixed, "rep", n_rep, offset)
        sequences.append(swap_gather(other, "tp", n_tp, 1))
    scale_hidden = lax.dynamic_slice_in_dim(scale_up, rep * hidden_width, hidden_width, 0)
    hidden = []
    for rows in sequences:
        rows = rms_rows(rows, ffn_gain)
        upward = dot(rows, up_all)
        hidden.append(jnp.square(jax.nn.relu(upward * scale_hidden)).astype(bf16))

    hidden = jnp.concatenate(hidden, axis=0)
    width = w_down.shape[1]
    per_tp = n_a // n_tp
    tp = lax.axis_index("tp")
    turn = ((lax.axis_index("fs") // factors[1]) // per_tp) ^ tp
    result = jnp.zeros((length, local_width), bf16)
    for y in range(factors[1]):
        for xi in range(per_tp):
            stacked = jnp.stack([down_rows[xt * per_tp + xi][y] for xt in range(n_tp)])
            blocks, block_scales = [], []
            for k in range(n_tp):
                blocks.append(lax.dynamic_index_in_dim(stacked, turn ^ k, 0, keepdims=False))
                origin = fs_origin(factors, xi, y) ^ ((turn ^ k) * per_tp * factors[1])
                block_scales.append(lax.dynamic_index_in_dim(scale_down, origin, 0, keepdims=False))
            both = jnp.concatenate(blocks, axis=1)
            partial = (dot(hidden, both) * jnp.concatenate(block_scales)).astype(bf16)
            total = partial[:, :width].astype(f32)
            for k in range(1, n_tp):
                pairs = [(i, i ^ k) for i in range(n_tp)]
                total = total + lax.ppermute(partial[:, k * width:(k + 1) * width], "tp", pairs).astype(f32)
            own = total[:length]
            for k in range(1, n_rep):
                back = shifted(total[k * length:(k + 1) * length].astype(bf16), "rep", n_rep, -k)
                own = own + back.astype(f32)
            inner = (fs_origin(factors, xi, y) % (per_tp * factors[1])) * width
            mixed_part = lax.dynamic_slice_in_dim(mixed, inner, width, 1)
            piece = (mixed_part.astype(f32) + own).astype(bf16)
            result = lax.dynamic_update_slice_in_dim(result, piece, inner, 1)
    return result[None]


def solution(mesh):
    n_rep, n_fs, n_tp = (mesh.shape[name] for name in ("rep", "fs", "tp"))

    def body(*args):
        return on_device(n_rep, n_fs, n_tp, *args)

    return jax.shard_map(
        body,
        mesh=mesh,
        in_specs=(
            P(("rep", "fs"), None, "tp"),
            P(),
            P("fs", "tp"),
            P(("tp", "fs")),
            P(),
            P("fs", "tp"),
            P(("tp", "fs")),
            P(),
            P("fs", "tp"),
            P(("tp", "fs")),
            P("tp", "fs"),
            P("fs"),
        ),
        out_specs=P(("rep", "fs"), None, "tp"),
        check_vma=False,
    )
```

time: 651 us -> 507 us (0.78)
  the two profiles are of different devices: /device:TPU:0 before, /device:TPU:18 now
where the time goes in v1:
time: 507 us; the launch traced here: 499 us
  waiting for transfers between devices  284 us (56%)
  matrix products  73.3 us (14%)
  local copies, waits for them, and re-layouts  64.5 us (13%)
  starting transfers between devices  47.2 us (9%)
  other arithmetic  28.8 us (6%)
    ppermute x35, waiting for transfers between devices, fs_sent(): return lax.ppermute(value, 'fs', pairs)  246 us
    dot_general x12, matrix products, dot(): return jnp.dot(left, right, preferred_element_type=f32)  72.9 us
    ppermute x35, starting transfers between devices, fs_sent(): return lax.ppermute(value, 'fs', pairs)  41.4 us
    ppermute x9, waiting for transfers between devices, shifted(): lax.ppermute(value, axis_name, [(i, (i + offset) % count) for i in range(...  38.6 us
    dynamic_update_slice x30, local copies, waits for them, and re-layouts, placed(): lax.dynamic_update_slice_in_dim(full, rows[x][y], fs_origin(factors, x, y...  34.9 us
  transfers between devices with their start and end apart: 48, of which 21 were waited for; matrix products, arithmetic and copies ran while one was open for 26% of the time, Pallas kernels for 0%

profile of v1, /device:TPU:18, one launch (start us, length us, event | category | flops | bytes accessed | tf_op | source)
XLA Modules:
  0.0 499.0 jit_solution(2236899819847353109)
XLA Ops:
  5.8 2.4 collective-permute-start.12
  13.0 1.7 dynamic-slice_convert_fusion
  15.7 1.6 constant_dynamic-update-slice_fusion.27
  17.4 4.4 broadcast_in_dim.85
  21.8 3.3 constant_dynamic-update-slice_fusion.11
  27.3 2.1 collective-permute-start.14
  29.4 2.9 copy.13
  37.0 2.8 collective-permute-start.1
  57.6 3.0 collective-permute-start.16
  65.2 1.6 constant_dynamic-update-slice_fusion.24
  68.9 2.9 collective-permute-start.24
  72.5 2.6 collective-permute-start.25
  79.3 3.2 collective-permute-done.5
  83.4 1.8 collective-permute-done.6
  86.2 2.1 collective-permute-done.7
  96.0 1.9 broadcast_select_fusion.5
  99.0 2.8 fusion.54
  101.8 2.3 fusion.20
  104.1 2.3 fusion.23
  106.5 2.4 fusion.26
  108.9 9.8 %collective-permute-done.22 = bf16[64,1024]{1,0:T(8,128)(2,1)S(1)} collective-permute-done((bf16[64,1024]{1,0:T(8,128)(2,1)S(1)}, bf16[64,1024]{1,0:T(8,128)(2,1)S(1)}, u32[]{:S(2)}, u32[]{:S(2)}) %collective-permute-start.22) | collective-permute-done | bytes 131104 | tf_op jit(solution)/shard_map/ppermute | solution.py:52
  118.7 1.9 collective-permute-start.36
  120.7 1.9 subtract_convert_fusion
  122.5 43.8 %collective-permute-done.25 = bf16[256,2048]{1,0:T(8,128)(2,1)S(1)} collective-permute-done((bf16[256,2048]{1,0:T(8,128)(2,1)}, bf16[256,2048]{1,0:T(8,128)(2,1)S(1)}, u32[]{:S(2)}, u32[]{:S(2)}) %collective-permute-start.25) | collective-permute-done | bytes 1048608 | tf_op jit(solution)/shard_map/ppermute | solution.py:52
  170.9 42.2 %collective-permute-done.26 = bf16[256,2048]{1,0:T(8,128)(2,1)S(1)} collective-permute-done((bf16[256,2048]{1,0:T(8,128)(2,1)}, bf16[256,2048]{1,0:T(8,128)(2,1)S(1)}, u32[]{:S(2)}, u32[]{:S(2)}) %collective-permute-start.26) | collective-permute-done | bytes 1048608 | tf_op jit(solution)/shard_map/ppermute | solution.py:52
  215.2 18.5 %collective-permute-done.33 = bf16[2048,256]{1,0:T(8,128)(2,1)S(1)} collective-permute-done((bf16[2048,256]{1,0:T(8,128)(2,1)S(1)}, bf16[2048,256]{1,0:T(8,128)(2,1)S(1)}, u32[]{:S(2)}, u32[]{:S(2)}) %collective-permute-start.33) | collective-permute-done | bytes 1048608 | tf_op jit(solution)/shard_map/ppermute | solution.py:52
  236.2 2.6 add_convert_fusion
  238.8 17.6 %collective-permute-done.37 = bf16[2048,256]{1,0:T(8,128)(2,1)S(1)} collective-permute-done((bf16[2048,256]{1,0:T(8,128)(2,1)S(1)}, bf16[2048,256]{1,0:T(8,128)(2,1)S(1)}, u32[]{:S(2)}, u32[]{:S(2)}) %collective-permute-start.37) | collective-permute-done | bytes 1048608 | tf_op jit(solution)/shard_map/ppermute | solution.py:52
  259.2 2.5 collective-permute-done.28
  262.2 21.9 %collective-permute-done.29 = bf16[256,2048]{1,0:T(8,128)(2,1)S(1)} collective-permute-done((bf16[256,2048]{1,0:T(8,128)(2,1)S(1)}, bf16[256,2048]{1,0:T(8,128)(2,1)S(1)}, u32[]{:S(2)}, u32[]{:S(2)}) %collective-permute-start.29) | collective-permute-done | bytes 1048608 | tf_op jit(solution)/shard_map/ppermute | solution.py:52
  284.7 21.9 %collective-permute-done.30 = bf16[256,2048]{1,0:T(8,128)(2,1)S(1)} collective-permute-done((bf16[256,2048]{1,0:T(8,128)(2,1)S(1)}, bf16[256,2048]{1,0:T(8,128)(2,1)S(1)}, u32[]{:S(2)}, u32[]{:S(2)}) %collective-permute-start.30) | collective-permute-done | bytes 1048608 | tf_op jit(solution)/shard_map/ppermute | solution.py:52
  312.0 17.0 %collective-permute-done.41 = bf16[2048,256]{1,0:T(8,128)(2,1)S(1)} collective-permute-done((bf16[2048,256]{1,0:T(8,128)(2,1)S(1)}, bf16[2048,256]{1,0:T(8,128)(2,1)S(1)}, u32[]{:S(2)}, u32[]{:S(2)}) %collective-permute-start.41) | collective-permute-done | bytes 1048608 | tf_op jit(solution)/shard_map/ppermute | solution.py:52
  329.1 22.5 %collective-permute-done.44 = bf16[2048,256]{1,0:T(8,128)(2,1)S(1)} collective-permute-done((bf16[2048,256]{1,0:T(8,128)(2,1)S(1)}, bf16[2048,256]{1,0:T(8,128)(2,1)S(1)}, u32[]{:S(2)}, u32[]{:S(2)}) %collective-permute-start.44) | collective-permute-done | bytes 1048608 | tf_op jit(solution)/shard_map/ppermute | solution.py:52
  351.5 18.2 %collective-permute-done.45 = bf16[2048,256]{1,0:T(8,128)(2,1)S(1)} collective-permute-done((bf16[2048,256]{1,0:T(8,128)(2,1)S(1)}, bf16[2048,256]{1,0:T(8,128)(2,1)S(1)}, u32[]{:S(2)}, u32[]{:S(2)}) %collective-permute-start.45) | collective-permute-done | bytes 1048608 | tf_op jit(solution)/shard_map/ppermute | solution.py:52
  369.7 2.6 fusion.60
  373.7 12.9 %multiply_convert_fusion.1 = bf16[1024,2048]{1,0:T(8,128)(2,1)S(1)} fusion(bf16[2048,2048]{1,0:T(8,128)(2,1)} %constant_dynamic-update-slice_fusion.4, f32[2048]{0:T(1024)S(1)} %dynamic_slice.73, f32[2048]{0:T(1024)S(1)} %copy-done.35, f32[1024]{0:T(1024)S(1)} %add_rsqrt_fusion.1, bf16[1024,1024]{0,1:T(8,128)(2,1)S(1)} %get-tuple-element.14, ...), kind=kOutput, calls=%fused_computation.17 | convolution fusion | flops 8613003264 | bytes 16797696 | tf_op jit(solution)/shard_map/dot_general | solution.py:15
  388.0 14.5 %multiply_convert_fusion = bf16[1024,2048]{1,0:T(8,128)(2,1)} fusion(bf16[2048,2048]{1,0:T(8,128)(2,1)} %constant_dynamic-update-slice_fusion.4, f32[1024]{0:T(1024)S(1)} %add_rsqrt_fusion, f32[2048]{0:T(1024)S(1)} %dynamic_slice.73, f32[2048]{0:T(1024)S(1)} %copy-done.35, bf16[1024,1024]{0,1:T(8,128)(2,1)S(1)} %get-tuple-element.16, ...), kind=kOutput, calls=%fused_computation.16 | convolution fusion | flops 8613003264 | bytes 16797696 | tf_op jit(solution)/shard_map/dot_general | solution.py:15
  402.6 6.8 %multiply_convert_fusion.5 = bf16[2048,512]{0,1:T(8,128)(2,1)S(1)} fusion(bf16[2048,256]{1,0:T(8,128)(2,1)S(1)} %get-tuple-element.30, bf16[2048,256]{1,0:T(8,128)(2,1)S(1)} %get-tuple-element.29, f32[512]{0:T(512)S(1)} %copy-done.32, bf16[1024,2048]{1,0:T(8,128)(2,1)} %multiply_convert_fusion, bf16[1024,2048]{1,0:T(8,128)(2,1)S(1)} %multiply_convert_fusion.1), kind=kOutput, calls=%fused_computation.33 | convolution fusion | flops 4318035968 | bytes 12584960 | tf_op jit(solution)/shard_map/dot_general | solution.py:15
  410.9 8.2 %multiply_convert_fusion.4 = bf16[2048,512]{0,1:T(8,128)(2,1)S(1)} fusion(bf16[2048,256]{1,0:T(8,128)(2,1)S(1)} %get-tuple-element.28, bf16[2048,256]{1,0:T(8,128)(2,1)S(1)} %get-tuple-element.27, f32[512]{0:T(512)S(1)} %copy-done.31, bf16[1024,2048]{1,0:T(8,128)(2,1)} %multiply_convert_fusion, bf16[1024,2048]{1,0:T(8,128)(2,1)} %copy-done.40), kind=kOutput, calls=%fused_computation.32 | convolution fusion | flops 4318035968 | bytes 12584960 | tf_op jit(solution)/shard_map/dot_general | solution.py:15
  420.2 8.2 %multiply_convert_fusion.3 = bf16[2048,512]{0,1:T(8,128)(2,1)S(1)} fusion(bf16[2048,256]{1,0:T(8,128)(2,1)S(1)} %copy-done.9, bf16[2048,256]{1,0:T(8,128)(2,1)S(1)} %copy-done.10, f32[512]{0:T(512)S(1)} %copy-done.30, bf16[1024,2048]{1,0:T(8,128)(2,1)} %multiply_convert_fusion, bf16[1024,2048]{1,0:T(8,128)(2,1)} %copy-done.40), kind=kOutput, calls=%fused_computation.31 | convolution fusion | flops 4318035968 | bytes 12584960 | tf_op jit(solution)/shard_map/dot_general | solution.py:15
  429.2 8.0 %multiply_convert_fusion.2 = bf16[2048,512]{0,1:T(8,128)(2,1)S(1)} fusion(bf16[2048,256]{1,0:T(8,128)(2,1)S(1)} %get-tuple-element.24, bf16[2048,256]{1,0:T(8,128)(2,1)S(1)} %get-tuple-element.23, f32[512]{0:T(512)S(1)} %copy-done.29, bf16[1024,2048]{1,0:T(8,128)(2,1)} %multiply_convert_fusion, bf16[1024,2048]{1,0:T(8,128)(2,1)} %copy-done.40), kind=kOutput, calls=%fused_computation.30 | convolution fusion | flops 4318035968 | bytes 12584960 | tf_op jit(solution)/shard_map/dot_general | solution.py:15
  437.4 1.6 convert_add_fusion.3
  440.5 1.6 convert_add_fusion.2
  449.7 5.3 %collective-permute-done.35 = bf16[1024,256]{0,1:T(8,128)(2,1)S(1)} collective-permute-done((bf16[1024,256]{0,1:T(8,128)(2,1)}, bf16[1024,256]{0,1:T(8,128)(2,1)S(1)}, u32[]{:S(2)}, u32[]{:S(2)}) %collective-permute-start.35) | collective-permute-done | bytes 524320 | tf_op jit(solution)/shard_map/ppermute | solution.py:25
  455.0 11.2 %collective-permute-done.39 = bf16[1024,256]{0,1:T(8,128)(2,1)S(1)} collective-permute-done((bf16[1024,256]{0,1:T(8,128)(2,1)}, bf16[1024,256]{0,1:T(8,128)(2,1)S(1)}, u32[]{:S(2)}, u32[]{:S(2)}) %collective-permute-start.39) | collective-permute-done | bytes 524320 | tf_op jit(solution)/shard_map/ppermute | solution.py:25
  466.2 11.3 %collective-permute-done.43 = bf16[1024,256]{0,1:T(8,128)(2,1)} collective-permute-done((bf16[1024,256]{0,1:T(8,128)(2,1)}, bf16[1024,256]{0,1:T(8,128)(2,1)}, u32[]{:S(2)}, u32[]{:S(2)}) %collective-permute-start.43) | collective-permute-done | bytes 524320 | tf_op jit(solution)/shard_map/ppermute | solution.py:25
  477.6 10.7 %collective-permute-done.47 = bf16[1024,256]{0,1:T(8,128)(2,1)} collective-permute-done((bf16[1024,256]{0,1:T(8,128)(2,1)}, bf16[1024,256]{0,1:T(8,128)(2,1)}, u32[]{:S(2)}, u32[]{:S(2)}) %collective-permute-start.47) | collective-permute-done | bytes 524320 | tf_op jit(solution)/shard_map/ppermute | solution.py:25
  488.3 5.0 fusion.86
  (238 shorter events, 97.9 us)
Async XLA Ops:
  0.8 26.0 %collective-permute-start.8 = (f32[1,928]{1,0:T(1,128)S(1)}, f32[1,928]{1,0:T(1,128)S(1)}, u32[]{:S(2)}, u32[]{:S(2)}) collective-permute-start(f32[1,928]{1,0:T(1,128)S(1)} %bitcast.77), channel_id=1, source_target_pairs={{0,4},{2,6},{4,0},{6,2},{8,12},{10,14},{12,8},{14,10},{1,5},{3,7},... | collective-permute-start | bytes 11144 | tf_op jit(solution)/shard_map/ppermute | solution.py:52
  2.4 24.8 %collective-permute-start.9 = (f32[1,928]{1,0:T(1,128)S(1)}, f32[1,928]{1,0:T(1,128)S(1)}, u32[]{:S(2)}, u32[]{:S(2)}) collective-permute-start(f32[1,928]{1,0:T(1,128)S(1)} %bitcast.78), channel_id=1, source_target_pairs={{0,8},{2,10},{4,12},{6,14},{8,0},{10,2},{12,4},{14,6},{1,9},{3,11}... | collective-permute-start | bytes 11144 | tf_op jit(solution)/shard_map/ppermute | solution.py:52
  2.7 34.3 %collective-permute-start.10 = (f32[1,928]{1,0:T(1,128)S(1)}, f32[1,928]{1,0:T(1,128)S(1)}, u32[]{:S(2)}, u32[]{:S(2)}) collective-permute-start(f32[1,928]{1,0:T(1,128)S(1)} %bitcast.79), channel_id=1, source_target_pairs={{0,12},{2,14},{4,8},{6,10},{8,4},{10,6},{12,0},{14,2},{1,13},{3,15... | collective-permute-start | bytes 11144 | tf_op jit(solution)/shard_map/ppermute | solution.py:52
  4.3 36.9 %collective-permute-start.11 = (f32[1,928]{1,0:T(1,128)S(1)}, f32[1,928]{1,0:T(1,128)S(1)}, u32[]{:S(2)}, u32[]{:S(2)}) collective-permute-start(f32[1,928]{1,0:T(1,128)S(1)} %bitcast.80), channel_id=1, source_target_pairs={{0,2},{2,0},{4,6},{6,4},{8,10},{10,8},{12,14},{14,12},{1,3},{3,1},... | collective-permute-start | bytes 11144 | tf_op jit(solution)/shard_map/ppermute | solution.py:52
  5.8 36.7 %collective-permute-start.12 = (f32[1,928]{1,0:T(1,128)S(1)}, f32[1,928]{1,0:T(1,128)S(1)}, u32[]{:S(2)}, u32[]{:S(2)}) collective-permute-start(f32[1,928]{1,0:T(1,128)S(1)} %bitcast.81), channel_id=1, source_target_pairs={{0,6},{2,4},{4,2},{6,0},{8,14},{10,12},{12,10},{14,8},{1,7},{3,5},... | collective-permute-start | bytes 11144 | tf_op jit(solution)/shard_map/ppermute | solution.py:52
  26.9 18.6 %collective-permute-start.13 = (f32[1,928]{1,0:T(1,128)S(1)}, f32[1,928]{1,0:T(1,128)}, u32[]{:S(2)}, u32[]{:S(2)}) collective-permute-start(f32[1,928]{1,0:T(1,128)S(1)} %bitcast.82), channel_id=1, source_target_pairs={{0,10},{2,8},{4,14},{6,12},{8,2},{10,0},{12,6},{14,4},{1,11},{3,9}... | collective-permute-start | bytes 11144 | tf_op jit(solution)/shard_map/ppermute | solution.py:52
  27.3 21.0 %collective-permute-start.14 = (f32[1,928]{1,0:T(1,128)S(1)}, f32[1,928]{1,0:T(1,128)}, u32[]{:S(2)}, u32[]{:S(2)}) collective-permute-start(f32[1,928]{1,0:T(1,128)S(1)} %bitcast.83), channel_id=1, source_target_pairs={{0,14},{2,12},{4,10},{6,8},{8,6},{10,4},{12,2},{14,0},{1,15},{3,13... | collective-permute-start | bytes 11144 | tf_op jit(solution)/shard_map/ppermute | solution.py:52
  37.0 20.5 %collective-permute-start.1 = (bf16[256,256]{1,0:T(8,128)(2,1)S(1)}, bf16[256,256]{1,0:T(8,128)(2,1)}, u32[]{:S(2)}, u32[]{:S(2)}) collective-permute-start(bf16[256,256]{1,0:T(8,128)(2,1)S(1)} %get-tuple-element.10), channel_id=1, source_target_pairs={{0,4},{2,6},{4,0},{6,2},{8,12},{10,14},{12,8},{14,10},{1,5},{3,7},... | collective-permute-start | bytes 393224 | tf_op jit(solution)/shard_map/ppermute | solution.py:52
  41.2 20.9 %collective-permute-start.2 = (bf16[256,256]{1,0:T(8,128)(2,1)S(1)}, bf16[256,256]{1,0:T(8,128)(2,1)}, u32[]{:S(2)}, u32[]{:S(2)}) collective-permute-start(bf16[256,256]{1,0:T(8,128)(2,1)S(1)} %get-tuple-element.10), channel_id=1, source_target_pairs={{0,8},{2,10},{4,12},{6,14},{8,0},{10,2},{12,4},{14,6},{1,9},{3,11}... | collective-permute-start | bytes 393224 | tf_op jit(solution)/shard_map/ppermute | solution.py:52
  42.6 21.1 %collective-permute-start.3 = (bf16[256,256]{1,0:T(8,128)(2,1)S(1)}, bf16[256,256]{1,0:T(8,128)(2,1)}, u32[]{:S(2)}, u32[]{:S(2)}) collective-permute-start(bf16[256,256]{1,0:T(8,128)(2,1)S(1)} %get-tuple-element.10), channel_id=1, source_target_pairs={{0,12},{2,14},{4,8},{6,10},{8,4},{10,6},{12,0},{14,2},{1,13},{3,15... | collective-permute-start | bytes 393224 | tf_op jit(solution)/shard_map/ppermute | solution.py:52
  45.4 21.3 %collective-permute-start.4 = (bf16[256,256]{1,0:T(8,128)(2,1)S(1)}, bf16[256,256]{1,0:T(8,128)(2,1)}, u32[]{:S(2)}, u32[]{:S(2)}) collective-permute-start(bf16[256,256]{1,0:T(8,128)(2,1)S(1)} %get-tuple-element.10), channel_id=1, source_target_pairs={{0,2},{2,0},{4,6},{6,4},{8,10},{10,8},{12,14},{14,12},{1,3},{3,1},... | collective-permute-start | bytes 393224 | tf_op jit(solution)/shard_map/ppermute | solution.py:52
  48.3 46.7 %collective-permute-start = (bf16[1024,1024]{0,1:T(8,128)(2,1)S(1)}, bf16[1024,1024]{0,1:T(8,128)(2,1)}, u32[]{:S(2)}, u32[]{:S(2)}) collective-permute-start(bf16[1024,1024]{0,1:T(8,128)(2,1)S(1)} %bitcast.65), channel_id=1, source_target_pairs={{0,1},{1,0},{2,3},{3,2},{4,5},{5,4},{6,7},{7,6},{8,9},{9,8},{10,11... | collective-permute-start | bytes 6291464 | tf_op jit(solution)/shard_map/ppermute | solution.py:25
  57.6 11.3 %collective-permute-start.16 = (bf16[64,1024]{1,0:T(8,128)(2,1)S(1)}, bf16[64,1024]{1,0:T(8,128)(2,1)S(1)}, u32[]{:S(2)}, u32[]{:S(2)}) collective-permute-start(bf16[64,1024]{1,0:T(8,128)(2,1)S(1)} %get-tuple-element.8), channel_id=1, source_target_pairs={{0,4},{2,6},{4,0},{6,2},{8,12},{10,14},{12,8},{14,10},{1,5},{3,7},... | collective-permute-start | bytes 393224 | tf_op jit(solution)/shard_map/ppermute | solution.py:52
  62.1 10.3 %collective-permute-start.17 = (bf16[64,1024]{1,0:T(8,128)(2,1)S(1)}, bf16[64,1024]{1,0:T(8,128)(2,1)S(1)}, u32[]{:S(2)}, u32[]{:S(2)}) collective-permute-start(bf16[64,1024]{1,0:T(8,128)(2,1)S(1)} %get-tuple-element.8), channel_id=1, source_target_pairs={{0,8},{2,10},{4,12},{6,14},{8,0},{10,2},{12,4},{14,6},{1,9},{3,11}... | collective-permute-start | bytes 393224 | tf_op jit(solution)/shard_map/ppermute | solution.py:52
  63.7 12.3 %collective-permute-start.18 = (bf16[64,1024]{1,0:T(8,128)(2,1)S(1)}, bf16[64,1024]{1,0:T(8,128)(2,1)S(1)}, u32[]{:S(2)}, u32[]{:S(2)}) collective-permute-start(bf16[64,1024]{1,0:T(8,128)(2,1)S(1)} %get-tuple-element.8), channel_id=1, source_target_pairs={{0,12},{2,14},{4,8},{6,10},{8,4},{10,6},{12,0},{14,2},{1,13},{3,15... | collective-permute-start | bytes 393224 | tf_op jit(solution)/shard_map/ppermute | solution.py:52
  66.8 10.4 %collective-permute-start.19 = (bf16[64,1024]{1,0:T(8,128)(2,1)S(1)}, bf16[64,1024]{1,0:T(8,128)(2,1)S(1)}, u32[]{:S(2)}, u32[]{:S(2)}) collective-permute-start(bf16[64,1024]{1,0:T(8,128)(2,1)S(1)} %get-tuple-element.8), channel_id=1, source_target_pairs={{0,2},{2,0},{4,6},{6,4},{8,10},{10,8},{12,14},{14,12},{1,3},{3,1},... | collective-permute-start | bytes 393224 | tf_op jit(solution)/shard_map/ppermute | solution.py:52
  68.9 49.8 %collective-permute-start.24 = (bf16[256,2048]{1,0:T(8,128)(2,1)}, bf16[256,2048]{1,0:T(8,128)(2,1)S(1)}, u32[]{:S(2)}, u32[]{:S(2)}) collective-permute-start(bf16[256,2048]{1,0:T(8,128)(2,1)} %get-tuple-element.12), channel_id=1, source_target_pairs={{0,4},{2,6},{4,0},{6,2},{8,12},{10,14},{12,8},{14,10},{1,5},{3,7},... | collective-permute-start | bytes 3145736 | tf_op jit(solution)/shard_map/ppermute | solution.py:52
  72.5 93.9 %collective-permute-start.25 = (bf16[256,2048]{1,0:T(8,128)(2,1)}, bf16[256,2048]{1,0:T(8,128)(2,1)S(1)}, u32[]{:S(2)}, u32[]{:S(2)}) collective-permute-start(bf16[256,2048]{1,0:T(8,128)(2,1)} %get-tuple-element.12), channel_id=1, source_target_pairs={{0,8},{2,10},{4,12},{6,14},{8,0},{10,2},{12,4},{14,6},{1,9},{3,11}... | collective-permute-start | bytes 3145736 | tf_op jit(solution)/shard_map/ppermute | solution.py:52
  76.0 6.6 %collective-permute-start.5 = (bf16[256,256]{1,0:T(8,128)(2,1)}, bf16[256,256]{1,0:T(8,128)(2,1)S(1)}, u32[]{:S(2)}, u32[]{:S(2)}) collective-permute-start(bf16[256,256]{1,0:T(8,128)(2,1)} %collective-permute-done.1), channel_id=1, source_target_pairs={{0,2},{2,0},{4,6},{6,4},{8,10},{10,8},{12,14},{14,12},{1,3},{3,1},... | collective-permute-start | bytes 393224 | tf_op jit(solution)/shard_map/ppermute | solution.py:52
  77.2 8.1 %collective-permute-start.6 = (bf16[256,256]{1,0:T(8,128)(2,1)}, bf16[256,256]{1,0:T(8,128)(2,1)S(1)}, u32[]{:S(2)}, u32[]{:S(2)}) collective-permute-start(bf16[256,256]{1,0:T(8,128)(2,1)} %collective-permute-done.2), channel_id=1, source_target_pairs={{0,2},{2,0},{4,6},{6,4},{8,10},{10,8},{12,14},{14,12},{1,3},{3,1},... | collective-permute-start | bytes 393224 | tf_op jit(solution)/shard_map/ppermute | solution.py:52
  82.5 5.8 %collective-permute-start.7 = (bf16[256,256]{1,0:T(8,128)(2,1)}, bf16[256,256]{1,0:T(8,128)(2,1)S(1)}, u32[]{:S(2)}, u32[]{:S(2)}) collective-permute-start(bf16[256,256]{1,0:T(8,128)(2,1)} %collective-permute-done.3), channel_id=1, source_target_pairs={{0,2},{2,0},{4,6},{6,4},{8,10},{10,8},{12,14},{14,12},{1,3},{3,1},... | collective-permute-start | bytes 393224 | tf_op jit(solution)/shard_map/ppermute | solution.py:52
  85.2 5.8 %collective-permute-start.20 = (bf16[64,1024]{1,0:T(8,128)(2,1)S(1)}, bf16[64,1024]{1,0:T(8,128)(2,1)S(1)}, u32[]{:S(2)}, u32[]{:S(2)}) collective-permute-start(bf16[64,1024]{1,0:T(8,128)(2,1)S(1)} %collective-permute-done.16), channel_id=1, source_target_pairs={{0,2},{2,0},{4,6},{6,4},{8,10},{10,8},{12,14},{14,12},{1,3},{3,1},... | collective-permute-start | bytes 393224 | tf_op jit(solution)/shard_map/ppermute | solution.py:52
  88.3 5.0 collective-permute-start.21
  91.1 122.1 %collective-permute-start.26 = (bf16[256,2048]{1,0:T(8,128)(2,1)}, bf16[256,2048]{1,0:T(8,128)(2,1)S(1)}, u32[]{:S(2)}, u32[]{:S(2)}) collective-permute-start(bf16[256,2048]{1,0:T(8,128)(2,1)} %get-tuple-element.12), channel_id=1, source_target_pairs={{0,12},{2,14},{4,8},{6,10},{8,4},{10,6},{12,0},{14,2},{1,13},{3,15... | collective-permute-start | bytes 3145736 | tf_op jit(solution)/shard_map/ppermute | solution.py:52
  93.3 120.4 %collective-permute-start.27 = (bf16[256,2048]{1,0:T(8,128)(2,1)}, bf16[256,2048]{1,0:T(8,128)(2,1)S(1)}, u32[]{:S(2)}, u32[]{:S(2)}) collective-permute-start(bf16[256,2048]{1,0:T(8,128)(2,1)} %get-tuple-element.12), channel_id=1, source_target_pairs={{0,2},{2,0},{4,6},{6,4},{8,10},{10,8},{12,14},{14,12},{1,3},{3,1},... | collective-permute-start | bytes 3145736 | tf_op jit(solution)/shard_map/ppermute | solution.py:52
  94.9 23.8 %collective-permute-start.22 = (bf16[64,1024]{1,0:T(8,128)(2,1)S(1)}, bf16[64,1024]{1,0:T(8,128)(2,1)S(1)}, u32[]{:S(2)}, u32[]{:S(2)}) collective-permute-start(bf16[64,1024]{1,0:T(8,128)(2,1)S(1)} %collective-permute-done.18), channel_id=1, source_target_pairs={{0,2},{2,0},{4,6},{6,4},{8,10},{10,8},{12,14},{14,12},{1,3},{3,1},... | collective-permute-start | bytes 393224 | tf_op jit(solution)/shard_map/ppermute | solution.py:52
  118.7 114.9 %collective-permute-start.33 = (bf16[2048,256]{1,0:T(8,128)(2,1)S(1)}, bf16[2048,256]{1,0:T(8,128)(2,1)S(1)}, u32[]{:S(2)}, u32[]{:S(2)}) collective-permute-start(bf16[2048,256]{1,0:T(8,128)(2,1)S(1)} %dynamic-slice_convert_fusion), channel_id=1, source_target_pairs={{0,8},{2,10},{4,12},{6,14},{8,0},{10,2},{12,4},{14,6},{1,9},{3,11}... | collective-permute-start | bytes 3145736 | tf_op jit(solution)/shard_map/ppermute | solution.py:52
  118.7 115.5 %collective-permute-start.36 = (bf16[2048,256]{1,0:T(8,128)(2,1)S(1)}, bf16[2048,256]{1,0:T(8,128)(2,1)S(1)}, u32[]{:S(2)}, u32[]{:S(2)}) collective-permute-start(bf16[2048,256]{1,0:T(8,128)(2,1)S(1)} %dynamic-slice_convert_fusion), channel_id=1, source_target_pairs={{0,4},{2,6},{4,0},{6,2},{8,12},{10,14},{12,8},{14,10},{1,5},{3,7},... | collective-permute-start | bytes 3145736 | tf_op jit(solution)/shard_map/ppermute | solution.py:52
  166.3 2.9 collective-permute-start.15
  169.3 87.1 %collective-permute-start.37 = (bf16[2048,256]{1,0:T(8,128)(2,1)S(1)}, bf16[2048,256]{1,0:T(8,128)(2,1)S(1)}, u32[]{:S(2)}, u32[]{:S(2)}) collective-permute-start(bf16[2048,256]{1,0:T(8,128)(2,1)S(1)} %dynamic-slice_convert_fusion), channel_id=1, source_target_pairs={{0,12},{2,14},{4,8},{6,10},{8,4},{10,6},{12,0},{14,2},{1,13},{3,15... | collective-permute-start | bytes 3145736 | tf_op jit(solution)/shard_map/ppermute | solution.py:52
  213.2 45.4 %collective-permute-start.40 = (bf16[2048,256]{1,0:T(8,128)(2,1)S(1)}, bf16[2048,256]{1,0:T(8,128)(2,1)S(1)}, u32[]{:S(2)}, u32[]{:S(2)}) collective-permute-start(bf16[2048,256]{1,0:T(8,128)(2,1)S(1)} %dynamic-slice_convert_fusion), channel_id=1, source_target_pairs={{0,2},{2,0},{4,6},{6,4},{8,10},{10,8},{12,14},{14,12},{1,3},{3,1},... | collective-permute-start | bytes 3145736 | tf_op jit(solution)/shard_map/ppermute | solution.py:52
  213.7 47.9 %collective-permute-start.28 = (bf16[256,2048]{1,0:T(8,128)(2,1)S(1)}, bf16[256,2048]{1,0:T(8,128)(2,1)S(1)}, u32[]{:S(2)}, u32[]{:S(2)}) collective-permute-start(bf16[256,2048]{1,0:T(8,128)(2,1)S(1)} %collective-permute-done.24), channel_id=1, source_target_pairs={{0,2},{2,0},{4,6},{6,4},{8,10},{10,8},{12,14},{14,12},{1,3},{3,1},... | collective-permute-start | bytes 3145736 | tf_op jit(solution)/shard_map/ppermute | solution.py:52
  233.6 50.5 %collective-permute-start.29 = (bf16[256,2048]{1,0:T(8,128)(2,1)S(1)}, bf16[256,2048]{1,0:T(8,128)(2,1)S(1)}, u32[]{:S(2)}, u32[]{:S(2)}) collective-permute-start(bf16[256,2048]{1,0:T(8,128)(2,1)S(1)} %collective-permute-done.25), channel_id=1, source_target_pairs={{0,2},{2,0},{4,6},{6,4},{8,10},{10,8},{12,14},{14,12},{1,3},{3,1},... | collective-permute-start | bytes 3145736 | tf_op jit(solution)/shard_map/ppermute | solution.py:52
  234.2 72.4 %collective-permute-start.30 = (bf16[256,2048]{1,0:T(8,128)(2,1)S(1)}, bf16[256,2048]{1,0:T(8,128)(2,1)S(1)}, u32[]{:S(2)}, u32[]{:S(2)}) collective-permute-start(bf16[256,2048]{1,0:T(8,128)(2,1)S(1)} %collective-permute-done.26), channel_id=1, source_target_pairs={{0,2},{2,0},{4,6},{6,4},{8,10},{10,8},{12,14},{14,12},{1,3},{3,1},... | collective-permute-start | bytes 3145736 | tf_op jit(solution)/shard_map/ppermute | solution.py:52
  256.4 115.9 %collective-permute-start.23 = (bf16[1024,1024]{0,1:T(8,128)(2,1)S(1)}, bf16[1024,1024]{0,1:T(8,128)(2,1)S(1)}, u32[]{:S(2)}, u32[]{:S(2)}) collective-permute-start(bf16[1024,1024]{0,1:T(8,128)(2,1)S(1)} %add_convert_fusion), channel_id=1, source_target_pairs={{0,1},{1,0},{2,3},{3,2},{4,5},{5,4},{6,7},{7,6},{8,9},{9,8},{10,11... | collective-permute-start | bytes 6291464 | tf_op jit(solution)/shard_map/ppermute | solution.py:25
  258.5 70.5 %collective-permute-start.41 = (bf16[2048,256]{1,0:T(8,128)(2,1)S(1)}, bf16[2048,256]{1,0:T(8,128)(2,1)S(1)}, u32[]{:S(2)}, u32[]{:S(2)}) collective-permute-start(bf16[2048,256]{1,0:T(8,128)(2,1)S(1)} %collective-permute-done.33), channel_id=1, source_target_pairs={{0,2},{2,0},{4,6},{6,4},{8,10},{10,8},{12,14},{14,12},{1,3},{3,1},... | collective-permute-start | bytes 3145736 | tf_op jit(solution)/shard_map/ppermute | solution.py:52
  261.7 89.9 %collective-permute-start.44 = (bf16[2048,256]{1,0:T(8,128)(2,1)S(1)}, bf16[2048,256]{1,0:T(8,128)(2,1)S(1)}, u32[]{:S(2)}, u32[]{:S(2)}) collective-permute-start(bf16[2048,256]{1,0:T(8,128)(2,1)S(1)} %collective-permute-done.36), channel_id=1, source_target_pairs={{0,2},{2,0},{4,6},{6,4},{8,10},{10,8},{12,14},{14,12},{1,3},{3,1},... | collective-permute-start | bytes 3145736 | tf_op jit(solution)/shard_map/ppermute | solution.py:52
  284.1 85.6 %collective-permute-start.45 = (bf16[2048,256]{1,0:T(8,128)(2,1)S(1)}, bf16[2048,256]{1,0:T(8,128)(2,1)S(1)}, u32[]{:S(2)}, u32[]{:S(2)}) collective-permute-start(bf16[2048,256]{1,0:T(8,128)(2,1)S(1)} %collective-permute-done.37), channel_id=1, source_target_pairs={{0,2},{2,0},{4,6},{6,4},{8,10},{10,8},{12,14},{14,12},{1,3},{3,1},... | collective-permute-start | bytes 3145736 | tf_op jit(solution)/shard_map/ppermute | solution.py:52
  306.6 67.0 %collective-permute-start.31 = (bf16[1024,1024]{0,1:T(8,128)(2,1)S(1)}, bf16[1024,1024]{0,1:T(8,128)(2,1)S(1)}, u32[]{:S(2)}, u32[]{:S(2)}) collective-permute-start(bf16[1024,1024]{0,1:T(8,128)(2,1)S(1)} %add_convert_fusion), channel_id=1, source_target_pairs={{0,16},{16,0},{1,17},{17,1},{2,18},{18,2},{3,19},{19,3},{4,20},{20... | collective-permute-start | bytes 6291464 | tf_op jit(solution)/shard_map/ppermute | solution.py:25
  373.6 13.1 %collective-permute-start.32 = (bf16[1024,1024]{0,1:T(8,128)(2,1)S(1)}, bf16[1024,1024]{0,1:T(8,128)(2,1)S(1)}, u32[]{:S(2)}, u32[]{:S(2)}) collective-permute-start(bf16[1024,1024]{0,1:T(8,128)(2,1)S(1)} %collective-permute-done.31), channel_id=1, source_target_pairs={{0,1},{1,0},{2,3},{3,2},{4,5},{5,4},{6,7},{7,6},{8,9},{9,8},{10,11... | collective-permute-start | bytes 6291464 | tf_op jit(solution)/shard_map/ppermute | solution.py:25
  410.4 27.0 %collective-permute-start.34 = (bf16[2048,256]{0,1:T(8,128)(2,1)}, bf16[2048,256]{0,1:T(8,128)(2,1)}, u32[]{:S(2)}, u32[]{:S(2)}) collective-permute-start(bf16[2048,256]{0,1:T(8,128)(2,1)} %slice.89), channel_id=1, source_target_pairs={{0,1},{1,0},{2,3},{3,2},{4,5},{5,4},{6,7},{7,6},{8,9},{9,8},{10,11... | collective-permute-start | bytes 3145736 | tf_op jit(solution)/shard_map/ppermute | solution.py:177
  420.2 20.3 %collective-permute-start.38 = (bf16[2048,256]{0,1:T(8,128)(2,1)}, bf16[2048,256]{0,1:T(8,128)(2,1)}, u32[]{:S(2)}, u32[]{:S(2)}) collective-permute-start(bf16[2048,256]{0,1:T(8,128)(2,1)} %slice.93), channel_id=1, source_target_pairs={{0,1},{1,0},{2,3},{3,2},{4,5},{5,4},{6,7},{7,6},{8,9},{9,8},{10,11... | collective-permute-start | bytes 3145736 | tf_op jit(solution)/shard_map/ppermute | solution.py:177
  428.6 15.9 %collective-permute-start.42 = (bf16[2048,256]{0,1:T(8,128)(2,1)S(1)}, bf16[2048,256]{0,1:T(8,128)(2,1)S(1)}, u32[]{:S(2)}, u32[]{:S(2)}) collective-permute-start(bf16[2048,256]{0,1:T(8,128)(2,1)S(1)} %slice.97), channel_id=1, source_target_pairs={{0,1},{1,0},{2,3},{3,2},{4,5},{5,4},{6,7},{7,6},{8,9},{9,8},{10,11... | collective-permute-start | bytes 3145736 | tf_op jit(solution)/shard_map/ppermute | solution.py:177
  437.3 9.0 %collective-permute-start.46 = (bf16[2048,256]{0,1:T(8,128)(2,1)S(1)}, bf16[2048,256]{0,1:T(8,128)(2,1)S(1)}, u32[]{:S(2)}, u32[]{:S(2)}) collective-permute-start(bf16[2048,256]{0,1:T(8,128)(2,1)S(1)} %slice.101), channel_id=1, source_target_pairs={{0,1},{1,0},{2,3},{3,2},{4,5},{5,4},{6,7},{7,6},{8,9},{9,8},{10,11... | collective-permute-start | bytes 3145736 | tf_op jit(solution)/shard_map/ppermute | solution.py:177
  440.0 15.0 %collective-permute-start.35 = (bf16[1024,256]{0,1:T(8,128)(2,1)}, bf16[1024,256]{0,1:T(8,128)(2,1)S(1)}, u32[]{:S(2)}, u32[]{:S(2)}) collective-permute-start(bf16[1024,256]{0,1:T(8,128)(2,1)} %slice.145), channel_id=1, source_target_pairs={{0,16},{16,0},{1,17},{17,1},{2,18},{18,2},{3,19},{19,3},{4,20},{20... | collective-permute-start | bytes 1572872 | tf_op jit(solution)/shard_map/ppermute | solution.py:25
  443.1 23.2 %collective-permute-start.39 = (bf16[1024,256]{0,1:T(8,128)(2,1)}, bf16[1024,256]{0,1:T(8,128)(2,1)S(1)}, u32[]{:S(2)}, u32[]{:S(2)}) collective-permute-start(bf16[1024,256]{0,1:T(8,128)(2,1)} %slice.144), channel_id=1, source_target_pairs={{0,16},{16,0},{1,17},{17,1},{2,18},{18,2},{3,19},{19,3},{4,20},{20... | collective-permute-start | bytes 1572872 | tf_op jit(solution)/shard_map/ppermute | solution.py:25
  445.8 31.8 %collective-permute-start.43 = (bf16[1024,256]{0,1:T(8,128)(2,1)}, bf16[1024,256]{0,1:T(8,128)(2,1)}, u32[]{:S(2)}, u32[]{:S(2)}) collective-permute-start(bf16[1024,256]{0,1:T(8,128)(2,1)} %slice.143), channel_id=1, source_target_pairs={{0,16},{16,0},{1,17},{17,1},{2,18},{18,2},{3,19},{19,3},{4,20},{20... | collective-permute-start | bytes 1572872 | tf_op jit(solution)/shard_map/ppermute | solution.py:25
  448.2 40.1 %collective-permute-start.47 = (bf16[1024,256]{0,1:T(8,128)(2,1)}, bf16[1024,256]{0,1:T(8,128)(2,1)}, u32[]{:S(2)}, u32[]{:S(2)}) collective-permute-start(bf16[1024,256]{0,1:T(8,128)(2,1)} %slice.142), channel_id=1, source_target_pairs={{0,16},{16,0},{1,17},{17,1},{2,18},{18,2},{3,19},{19,3},{4,20},{20... | collective-permute-start | bytes 1572872 | tf_op jit(solution)/shard_map/ppermute | solution.py:25
  (41 other events, 778.7 us)
